TPU v7x, 128 devices: a whole 4x4x4 slice. The times are simulated.
128 devices in a mesh: sp: 16 (over z, y), tp: 8 (over x, core).
Axes of the slice: x: 4, y: 4, z: 4, core: 2. Of those that a mesh axis runs over, the one named last changes fastest.
Arguments:
- layer_input: bfloat16 [16, 4096, 2048], P(None, ('sp', 'tp')), may hold values from -6 to 6
- input_gain: float32 [2048], replicated, may hold values from 0.5 to 1.5
- narrowing_matrix: bfloat16 [2048, 512], replicated, may hold values from -0.125 to 0.125
- rotary_down: bfloat16 [2048, 64], replicated, may hold values from -0.125 to 0.125
- summary_scaling: float32 [512], replicated, may hold values from 0.5 to 1.5
- lookup_widening: bfloat16 [512, 16, 128], P('tp'), may hold values from -0.25 to 0.25
- payload_widening: bfloat16 [512, 16, 128], P('tp'), may hold values from -0.25 to 0.25
- query_nope: bfloat16 [16, 16, 128], P('sp', 'tp'), may hold values from -6 to 6
- query_rotary: bfloat16 [16, 16, 64], P('sp', 'tp'), may hold values from -6 to 6
Outputs:
- stored_summaries: bfloat16 [16, 4096, 512], P('sp', None, 'tp')
- rotary_cache: bfloat16 [16, 4096, 64], P('sp', None, 'tp')
- first_read: bfloat16 [16, 16, 128], P('sp', 'tp')
All inputs are finite; a program needn't handle non-finite values.
Results may differ from a plain program's by a relative error of at most 0.02.
Values may be sent and summed in bfloat16 or wider, within the bound.
A program may use at most 64 MiB of HBM per device.

v0:
```python
import jax
import jax.numpy as jnp
from jax import lax
from jax.sharding import Mesh
from jax.sharding import PartitionSpec as P

QK_ROPE = 64
PLAIN_MATCH_SPAN = 128
TP = ("tp_0", "tp_1")
SP_TP = ("sp", "tp_0", "tp_1")
norm_eps = 1e-06
rotary_base = 10000.0


def joined_along(parts, dim):
    parts = jnp.moveaxis(parts, 0, dim)
    lengths = parts.shape
    return parts.reshape(*lengths[:dim], lengths[dim] * lengths[dim + 1], *lengths[dim + 2 :])


def gather_together(arrays, axis, dims):
    line = jnp.concatenate([a.reshape(-1) for a in arrays])
    lines, at, finished = (lax.all_gather(line, axis), 0, [])
    for a, dim in zip(arrays, dims):
        parts = lines[:, at : at + a.size].reshape(-1, *a.shape)
        finished.append(joined_along(parts, dim))
        at += a.size
    return tuple(finished)


def total_of_pieces(array, axis):
    parts = lax.all_gather(array, axis).astype(jnp.float32)
    return parts.sum(axis=0)


def summed_rows(term, width, axes):
    subtotal = term(jnp.int32(0), width * lax.axis_size(axes))
    for axis in axes:
        subtotal = lax.psum_scatter(subtotal, axis, scatter_dimension=0, tiled=True)
    return subtotal


def rescaled_lines(vector):
    return vector * lax.rsqrt(jnp.mean(vector * vector, axis=-1, keepdims=True) + norm_eps)


def rotate(vector, position):
    half_width = vector.shape[-1] // 2
    frequency = 1.0 / rotary_base ** (
        jnp.arange(half_width, dtype=jnp.float32) * 2.0 / vector.shape[-1]
    )
    angles = position * frequency
    first_half = vector[..., :half_width]
    second_half = vector[..., half_width:]
    return jnp.concatenate(
        [
            first_half * jnp.cos(angles) - second_half * jnp.sin(angles),
            second_half * jnp.cos(angles) + first_half * jnp.sin(angles),
        ],
        axis=-1,
    )


def to_pieces(array, sp_count, tp_count):
    seq_count, pos_local, cache_width = array.shape
    seq_each = seq_count // sp_count
    width_each = cache_width // tp_count
    array = array.reshape(sp_count, seq_each, pos_local, tp_count, width_each)
    array = array.transpose(0, 3, 1, 2, 4)
    return array.reshape(sp_count * tp_count, seq_each, pos_local, width_each)


def shards(
    layer_input,
    input_gain,
    narrowing_matrix,
    rotary_down,
    summary_scaling,
    lookup_widening,
    payload_widening,
    query_nope,
    query_rotary,
):
    seq_count, pos_local, feature_width = layer_input.shape
    sp_count = lax.axis_size("sp")
    tp_count = lax.axis_size(TP)
    block_index = lax.axis_index(SP_TP)
    normed = (rescaled_lines(layer_input.astype(jnp.float32)) * input_gain).astype(jnp.bfloat16)
    flat_rows = normed.reshape(seq_count * pos_local, feature_width)
    hidden_summary = jnp.dot(
        flat_rows, narrowing_matrix, preferred_element_type=jnp.float32
    ).astype(jnp.bfloat16)
    rotary = jnp.dot(flat_rows, rotary_down, preferred_element_type=jnp.float32).astype(
        jnp.bfloat16
    )
    hidden_summary = (
        (rescaled_lines(hidden_summary.astype(jnp.float32)) * summary_scaling)
        .astype(jnp.bfloat16)
        .reshape(seq_count, pos_local, -1)
    )
    positions = (block_index * pos_local + jnp.arange(pos_local, dtype=jnp.int32)).astype(
        jnp.float32
    )[None, :, None]
    rotary = rotate(rotary.astype(jnp.float32).reshape(seq_count, pos_local, -1), positions).astype(
        jnp.bfloat16
    )
    moved = (
        lax.all_to_all(
            to_pieces(hidden_summary, sp_count, tp_count),
            SP_TP,
            split_axis=0,
            concat_axis=2,
            tiled=True,
        ),
        lax.all_to_all(
            to_pieces(rotary, sp_count, tp_count), SP_TP, split_axis=0, concat_axis=2, tiled=True
        ),
    )
    hidden_summary = moved[0][0]
    rotary = moved[1][0]
    pos_total = hidden_summary.shape[1]
    rot_each = rotary.shape[2]
    head_each = query_nope.shape[1]
    query_all, turn_all = gather_together((query_nope, query_rotary), TP, (1, 1))
    absorbed = jnp.einsum(
        "shd,chd->shc", query_all, lookup_widening, preferred_element_type=jnp.float32
    ).astype(jnp.bfloat16)
    query_turned = rotate(turn_all.astype(jnp.float32), jnp.float32(pos_total)).astype(jnp.bfloat16)
    turned_mine = lax.dynamic_slice_in_dim(query_turned, lax.axis_index(TP) * rot_each, rot_each, 2)
    score_scale = (PLAIN_MATCH_SPAN + QK_ROPE) ** (-0.5)
    partial_value = (
        jnp.einsum("shc,spc->shp", absorbed, hidden_summary, preferred_element_type=jnp.float32)
        + jnp.einsum("shr,spr->shp", turned_mine, rotary, preferred_element_type=jnp.float32)
    ) * score_scale
    scores = total_of_pieces(partial_value.astype(jnp.bfloat16), TP).astype(jnp.float32)
    attention = jax.nn.softmax(scores, axis=-1).astype(jnp.bfloat16)
    context = jnp.einsum(
        "shp,spc->shc", attention, hidden_summary, preferred_element_type=jnp.float32
    ).astype(jnp.bfloat16)

    def project_heads(row_start, row_count):
        part_context = lax.dynamic_slice_in_dim(context, row_start, row_count, 1)
        part_weight = lax.dynamic_slice_in_dim(payload_widening, row_start, row_count, 1)
        return jnp.einsum(
            "shc,chv->hsv", part_context, part_weight, preferred_element_type=jnp.float32
        )

    values = summed_rows(project_heads, head_each, TP)
    first_read = rescaled_lines(values.transpose(1, 0, 2)).astype(jnp.bfloat16)
    return (hidden_summary, rotary, first_read)


def solution(mesh):
    torus = Mesh(mesh.devices.reshape(mesh.shape["sp"], 4, 2), ("sp", "tp_0", "tp_1"))
    in_specs = (
        P(None, SP_TP, None),
        P(),
        P(),
        P(),
        P(),
        P(TP, None, None),
        P(TP, None, None),
        P("sp", TP, None),
        P("sp", TP, None),
    )
    out_specs = (P("sp", None, TP), P("sp", None, TP), P("sp", TP, None))
    return jax.shard_map(
        shards, mesh=torus, in_specs=in_specs, out_specs=out_specs, check_vma=False
    )
```

profile of v0, /device:TPU:1, one launch (start us, length us, event | category | flops | bytes accessed | tf_op | source)
XLA Modules:
  0.0 115.7 jit_solution(14926533977251242927)
XLA Ops:
  7.2 2.2 %fusion.2 = f32[16,32]{1,0:T(8,128)S(1)} fusion(bf16[16,32,2048]{2,1,0:T(8,128)(2,1)} %param.9), kind=kLoop, calls=%fused_computation.5 | loop fusion | flops 3145216 | bytes 2099200 | tf_op jit(solution)/shard_map/reduce_sum | solution.py:44
  10.1 1.3 %copy-done.2 = bf16[16,32,2048]{2,1,0:T(8,128)(2,1)} copy-done((bf16[16,32,2048]{2,1,0:T(8,128)(2,1)}, bf16[16,32,2048]{2,1,0:T(8,128)(2,1)S(1)}, u32[]{:S(2)}) %copy-start.2) | copy-done | bytes 2097176
  11.5 0.8 fusion.5
  13.0 0.8 reshape.408
  13.8 11.5 %all-to-all-start.1 = ((bf16[128,2,128]{2,1,0:T(2,128)(2,1)}), bf16[128,2,128]{2,1,0:T(2,128)(2,1)S(1)}, u32[]{:S(2)}, u32[]{:S(2)}) async-start(bf16[128,2,128]{2,1,0:T(2,128)(2,1)} %reshape.408), calls=%async_computation.1 | async-start | bytes 131072 | tf_op jit(solution)/shard_map/all_to_all | solution.py:115
  25.4 12.3 %all-gather.2 = bf16[8,1,384]{2,1,0:T(2,128)(2,1)S(1)} all-gather(bf16[1,1,384]{2,1,0:T(2,128)(2,1)S(1)} %reshape.390), channel_id=2, replica_groups=mesh['sp'=16,'tp_0'=4,'tp_1'=2] {'tp_0','tp_1'}, dimensions={0}, use_global_device_ids=true | all-gather | bytes 6912 | tf_op jit(solution)/shard_map/all_gather | solution.py:23
  37.7 2.9 %fusion.7 = (f32[512]{0:T(512)S(1)}, bf16[512,512]{0,1:T(8,128)(2,1)S(1)}) fusion(bf16[512,2048]{1,0:T(8,128)(2,1)} %bitcast.76, bf16[2048,512]{1,0:T(8,128)(2,1)S(1)} %copy-done), kind=kOutput, calls=%fused_computation.16 | convolution fusion | flops 1074789888 | bytes 4720640 | tf_op jit(solution)/shard_map/dot_general | solution.py:90
  40.9 1.0 copy.36
  41.9 1.6 %reshape_reshape.3 = bf16[16,1,32,8,64]{4,3,2,0,1:T(8,128)(2,1)S(1)} reshape(bf16[512,512]{1,0:T(8,128)(2,1)} %copy.36) | data formatting | bytes 1048576 | tf_op jit(solution)/shard_map/reshape;reshape | solution.py:68
  43.5 1.2 %copy.37 = bf16[16,8,1,32,64]{4,3,1,0,2:T(8,128)(2,1)} copy(bf16[16,8,1,32,64]{4,1,3,0,2:T(8,128)(2,1)S(1)} %bitcast.77) | data formatting | bytes 1048576 | tf_op jit(solution)/shard_map/transpose | solution.py:69
  44.7 3.0 %reshape.406 = bf16[128,2,1024]{2,1,0:T(2,128)(2,1)} reshape(bf16[128,1,32,64]{3,2,1,0:T(8,128)(2,1)} %bitcast.78) | data formatting | bytes 1048576
  47.8 8.9 %all-to-all-start = ((bf16[128,2,1024]{2,1,0:T(2,128)(2,1)}), bf16[128,2,1024]{2,1,0:T(2,128)(2,1)}, u32[]{:S(2)}, u32[]{:S(2)}) async-start(bf16[128,2,1024]{2,1,0:T(2,128)(2,1)} %reshape.406), calls=%async_computation | async-start | bytes 1048576 | tf_op jit(solution)/shard_map/all_to_all | solution.py:108
  57.6 12.3 %all-to-all-done = bf16[128,2,1024]{2,1,0:T(2,128)(2,1)} async-done(((bf16[128,2,1024]{2,1,0:T(2,128)(2,1)}), bf16[128,2,1024]{2,1,0:T(2,128)(2,1)}, u32[]{:S(2)}, u32[]{:S(2)}) %all-to-all-start) | async-done | bytes 524320 | tf_op jit(solution)/shard_map/all_to_all | solution.py:108
  69.9 2.3 %reshape.407 = bf16[128,1,32,64]{3,2,1,0:T(8,128)(2,1)S(1)} reshape(bf16[128,2,1024]{2,1,0:T(2,128)(2,1)} %all-to-all-done) | data formatting | bytes 1048576
  72.6 0.9 fusion.1
  73.5 0.6 dynamic-slice.2
  76.0 0.9 squeeze.7
  76.9 1.1 copy.45
  78.0 15.5 %all-gather.5.cloned.1.call-done = bf16[128,4096]{1,0:T(8,128)(2,1)} async-done(((bf16[16,4096]{1,0:T(8,128)(2,1)}), bf16[128,4096]{1,0:T(8,128)(2,1)}) %all-gather.5.cloned.1.call-update) | async-done | bytes 1048592 | tf_op jit(solution)/shard_map/all_gather | solution.py:32
  93.6 1.4 %convert_reduce_fusion = f32[16,4096]{1,0:T(8,128)S(1)} fusion(bf16[8,16,4096]{2,1,0:T(8,128)(2,1)} %bitcast.80), kind=kLoop, calls=%fused_computation.8 | loop fusion | flops 983040 | bytes 1310720 | tf_op jit(solution)/shard_map/reduce_sum | solution.py:33
  95.7 1.1 fusion.13
  96.8 6.9 %all-reduce = f32[16,1,128]{2,0,1:T(8,128)S(1)} all-reduce(f32[16,1,128]{2,0,1:T(8,128)S(1)} %bitcast.86), channel_id=4, replica_groups=mesh['sp'=16,'tp_0'=4,'tp_1'=2] {'tp_0'}, use_global_device_ids=true, to_apply=%region_5.0.clone | all-reduce | flops 2048 | bytes 16384
  103.7 4.4 %all-reduce.1 = f32[4,1,128]{2,0,1:T(4,128)S(1)} all-reduce(f32[4,1,128]{2,0,1:T(4,128)S(1)} %constant_dynamic-slice_fusion), channel_id=5, replica_groups=mesh['sp'=16,'tp_0'=4,'tp_1'=2] {'tp_1'}, use_global_device_ids=true, to_apply=%region_6.0.clone | all-reduce | flops 512 | bytes 4096
  108.3 0.6 multiply_convert_fusion
  (57 shorter events, 4.5 us)
Async XLA Ops:
  7.2 30.5 %copy-start = (bf16[2048,512]{1,0:T(8,128)(2,1)S(1)}, bf16[2048,512]{1,0:T(8,128)(2,1)}, u32[]{:S(2)}) copy-start(bf16[2048,512]{1,0:T(8,128)(2,1)} %param.11) | copy-start | bytes 6291460
  7.2 2.3 %copy-start.4 = (f32[2048]{0:T(1024)S(1)}, f32[2048]{0:T(1024)}, u32[]{:S(2)}) copy-start(f32[2048]{0:T(1024)} %param.10) | copy-start | bytes 24580
  7.2 2.3 %copy-start.1 = (bf16[16,32,2048]{2,1,0:T(8,128)(2,1)S(1)}, bf16[16,32,2048]{2,1,0:T(8,128)(2,1)}, u32[]{:S(2)}) copy-start(bf16[16,32,2048]{2,1,0:T(8,128)(2,1)} %param.9) | copy-start | bytes 6291460
  9.6 1.9 %copy-start.3 = (bf16[2048,64]{0,1:T(8,128)(2,1)S(1)}, bf16[2048,64]{0,1:T(8,128)(2,1)}, u32[]{:S(2)}) copy-start(bf16[2048,64]{0,1:T(8,128)(2,1)} %param.12) | copy-start | bytes 786436
  10.1 1.4 %copy-start.2 = (bf16[16,32,2048]{2,1,0:T(8,128)(2,1)}, bf16[16,32,2048]{2,1,0:T(8,128)(2,1)S(1)}, u32[]{:S(2)}) copy-start(bf16[16,32,2048]{2,1,0:T(8,128)(2,1)S(1)} %fusion.4) | copy-start | bytes 6291460
  11.5 13.8 %copy-start.8 = (bf16[1,2,64]{2,1,0:T(2,128)(2,1)S(1)}, bf16[1,2,64]{2,1,0:T(2,128)(2,1)}, u32[]{:S(2)}) copy-start(bf16[1,2,64]{2,1,0:T(2,128)(2,1)} %param.17) | copy-start | bytes 772
  11.5 13.9 %copy-start.6 = (bf16[1,2,128]{2,1,0:T(2,128)(2,1)S(1)}, bf16[1,2,128]{2,1,0:T(2,128)(2,1)}, u32[]{:S(2)}) copy-start(bf16[1,2,128]{2,1,0:T(2,128)(2,1)} %param.16) | copy-start | bytes 1540
  13.8 34.0 %all-to-all-start.1 = ((bf16[128,2,128]{2,1,0:T(2,128)(2,1)}), bf16[128,2,128]{2,1,0:T(2,128)(2,1)S(1)}, u32[]{:S(2)}, u32[]{:S(2)}) async-start(bf16[128,2,128]{2,1,0:T(2,128)(2,1)} %reshape.408), calls=%async_computation.1 | async-start | bytes 131072 | tf_op jit(solution)/shard_map/all_to_all | solution.py:115
  37.6 2.9 %copy-start.5 = (f32[512]{0:T(512)S(1)}, f32[512]{0:T(512)}, u32[]{:S(2)}) copy-start(f32[512]{0:T(512)} %param.13) | copy-start | bytes 6148
  44.7 12.1 %copy-start.7 = (bf16[64,16,128]{2,1,0:T(8,128)(2,1)S(1)}, bf16[64,16,128]{2,1,0:T(8,128)(2,1)}, u32[]{:S(2)}) copy-start(bf16[64,16,128]{2,1,0:T(8,128)(2,1)} %param.14) | copy-start | bytes 786436
  47.8 22.2 %all-to-all-start = ((bf16[128,2,1024]{2,1,0:T(2,128)(2,1)}), bf16[128,2,1024]{2,1,0:T(2,128)(2,1)}, u32[]{:S(2)}, u32[]{:S(2)}) async-start(bf16[128,2,1024]{2,1,0:T(2,128)(2,1)} %reshape.406), calls=%async_computation | async-start | bytes 1048576 | tf_op jit(solution)/shard_map/all_to_all | solution.py:108
  56.7 36.9 %all-gather.5.cloned.1.call-start = ((), (), s32[]{:S(2)}) async-start(), calls=%async_computation.2 | async-start | bytes 1179648 | tf_op jit(solution)/shard_map/all_gather | solution.py:32
  57.3 16.2 %copy-start.10 = (u32[128]{0:T(128)S(1)}, u32[128]{0:T(128)}, u32[]{:S(2)}) copy-start(u32[128]{0:T(128)} %constant.62) | copy-start | bytes 1540
  57.3 16.8 %copy-start.9 = (u32[128]{0:T(128)S(1)}, u32[128]{0:T(128)}, u32[]{:S(2)}) copy-start(u32[128]{0:T(128)} %constant.58) | copy-start | bytes 1540
Sparse Core Ops, SparseCore 0:
  73.6 19.8 all-gather.4
where the time goes:
time: 116 us
  waiting for transfers between devices  27.9 us (24%)
  blocking collectives  23.6 us (20%)
  starting transfers between devices  20.4 us (18%)
  local copies, waits for them, and re-layouts  15.6 us (13%)
  between operations  15.6 us (13%)
  matrix products  6.64 us (6%)
  other arithmetic  5.98 us (5%)
    all_gather x1, waiting for transfers between devices, total_of_pieces(): parts = lax.all_gather(array, axis).astype(jnp.float32)  15.5 us
    all_to_all x1, waiting for transfers between devices, shards(): lax.all_to_all(to_pieces(hidden_summary, sp_count, tp_count), SP_TP, spli...  12.3 us
    all_gather x1, blocking collectives, gather_together(): lines, at, finished = (lax.all_gather(line, axis), 0, [])  12.3 us
    all_to_all x1, starting transfers between devices, shards(): lax.all_to_all(to_pieces(rotary, sp_count, tp_count), SP_TP, split_axis=0...  11.5 us
    unnamed x2, blocking collectives  11.3 us
    unnamed x32, local copies, waits for them, and re-layouts  10.1 us
    all_to_all x1, starting transfers between devices, shards(): lax.all_to_all(to_pieces(hidden_summary, sp_count, tp_count), SP_TP, spli...  8.91 us
    dot_general x1, matrix products, shards(): jnp.dot(flat_rows, narrowing_matrix, preferred_element_type=jnp.float32)  2.9 us
  transfers between devices with their start and end apart: 3, of which 2 were waited for; matrix products, arithmetic and copies ran while one was open for 12% of the time, Pallas kernels for 0%

commit v1 on v0

--- a/solution.py
+++ b/solution.py
@@ -105,12 +105,18 @@
         jnp.bfloat16
     )
     moved = (
-        lax.all_to_all(
-            to_pieces(hidden_summary, sp_count, tp_count),
-            SP_TP,
-            split_axis=0,
-            concat_axis=2,
-            tiled=True,
+        jnp.concatenate(
+            lax.all_to_all(
+                jnp.stack(
+                    jnp.split(
+                        to_pieces(hidden_summary, sp_count, tp_count), lax.axis_size(SP_TP), axis=0
+                    )
+                ),
+                axis_name=SP_TP,
+                split_axis=0,
+                concat_axis=0,
+            ),
+            axis=2,
         ),
         lax.all_to_all(
             to_pieces(rotary, sp_count, tp_count), SP_TP, split_axis=0, concat_axis=2, tiled=True

time: 116 us -> 115 us (level)
  local copies, waits for them, and re-layouts: 15.6 us -> 14.1 us
    unnamed x32 -> x157, local copies, waits for them, and re-layouts: 10.1 us -> 9.53 us
where the time goes in v1:
time: 115 us
  waiting for transfers between devices  26.9 us (23%)
  blocking collectives  23.6 us (21%)
  starting transfers between devices  20.4 us (18%)
  between operations  16 us (14%)
  local copies, waits for them, and re-layouts  14.1 us (12%)
  matrix products  7.59 us (7%)
  other arithmetic  5.98 us (5%)
    all_gather x1, waiting for transfers between devices, total_of_pieces(): parts = lax.all_gather(array, axis).astype(jnp.float32)  15.5 us
    all_gather x1, blocking collectives, gather_together(): lines, at, finished = (lax.all_gather(line, axis), 0, [])  12.3 us
    all_to_all x1, starting transfers between devices, shards(): lax.all_to_all(to_pieces(rotary, sp_count, tp_count), SP_TP, split_axis=0...  11.5 us
    all_to_all x1, waiting for transfers between devices, shards(): lax.all_to_all(jnp.stack(jnp.split(to_pieces(hidden_summary, sp_count, tp...  11.4 us
    unnamed x2, blocking collectives  11.3 us
    unnamed x157, local copies, waits for them, and re-layouts  9.53 us
    all_to_all x1, starting transfers between devices, shards(): lax.all_to_all(jnp.stack(jnp.split(to_pieces(hidden_summary, sp_count, tp...  8.91 us
    dot_general x1, matrix products, shards(): jnp.dot(flat_rows, narrowing_matrix, preferred_element_type=jnp.float32)  2.9 us
  transfers between devices with their start and end apart: 3, of which 2 were waited for; matrix products, arithmetic and copies ran while one was open for 12% of the time, Pallas kernels for 0%

profile of v1, /device:TPU:1, one launch (start us, length us, event | category | flops | bytes accessed | tf_op | source)
XLA Modules:
  0.0 114.6 jit_solution(15294480907791573287)
XLA Ops:
  7.2 2.2 %fusion.2 = f32[16,32]{1,0:T(8,128)S(1)} fusion(bf16[16,32,2048]{2,1,0:T(8,128)(2,1)} %param.9), kind=kLoop, calls=%fused_computation.5 | loop fusion | flops 3145216 | bytes 2099200 | tf_op jit(solution)/shard_map/reduce_sum | solution.py:44
  10.1 1.3 %copy-done.2 = bf16[16,32,2048]{2,1,0:T(8,128)(2,1)} copy-done((bf16[16,32,2048]{2,1,0:T(8,128)(2,1)}, bf16[16,32,2048]{2,1,0:T(8,128)(2,1)S(1)}, u32[]{:S(2)}) %copy-start.2) | copy-done | bytes 2097176
  11.5 0.8 fusion.5
  13.0 0.8 reshape.404
  13.8 11.5 %all-to-all-start.1 = ((bf16[128,2,128]{2,1,0:T(2,128)(2,1)}), bf16[128,2,128]{2,1,0:T(2,128)(2,1)S(1)}, u32[]{:S(2)}, u32[]{:S(2)}) async-start(bf16[128,2,128]{2,1,0:T(2,128)(2,1)} %reshape.404), calls=%async_computation.1 | async-start | bytes 131072 | tf_op jit(solution)/shard_map/all_to_all | solution.py:121
  25.4 12.3 %all-gather.2 = bf16[8,1,384]{2,1,0:T(2,128)(2,1)S(1)} all-gather(bf16[1,1,384]{2,1,0:T(2,128)(2,1)S(1)} %reshape.386), channel_id=2, replica_groups=mesh['sp'=16,'tp_0'=4,'tp_1'=2] {'tp_0','tp_1'}, dimensions={0}, use_global_device_ids=true | all-gather | bytes 6912 | tf_op jit(solution)/shard_map/all_gather | solution.py:23
  37.7 2.9 %fusion.7 = (f32[512]{0:T(512)S(1)}, bf16[512,512]{0,1:T(8,128)(2,1)S(1)}) fusion(bf16[512,2048]{1,0:T(8,128)(2,1)} %bitcast.713, bf16[2048,512]{1,0:T(8,128)(2,1)S(1)} %copy-done), kind=kOutput, calls=%fused_computation.16 | convolution fusion | flops 1074789888 | bytes 4720640 | tf_op jit(solution)/shard_map/dot_general | solution.py:90
  40.7 1.0 copy.540
  41.8 1.6 %reshape_reshape.3 = bf16[16,1,32,8,64]{4,3,2,0,1:T(8,128)(2,1)S(1)} reshape(bf16[512,512]{1,0:T(8,128)(2,1)} %copy.540) | data formatting | bytes 1048576 | tf_op jit(solution)/shard_map/reshape;reshape | solution.py:68
  45.3 1.4 %reshape.402 = bf16[128,2,1024]{2,1,0:T(2,128)(2,1)} reshape(bf16[128,1,1,32,64]{4,3,2,1,0:T(8,128)(2,1)S(1)} %constant_dynamic-update-slice_fusion) | data formatting | bytes 1048576
  46.7 8.9 %all-to-all-start = ((bf16[128,2,1024]{2,1,0:T(2,128)(2,1)}), bf16[128,2,1024]{2,1,0:T(2,128)(2,1)}, u32[]{:S(2)}, u32[]{:S(2)}) async-start(bf16[128,2,1024]{2,1,0:T(2,128)(2,1)} %reshape.402), calls=%async_computation | async-start | bytes 1048576 | tf_op jit(solution)/shard_map/all_to_all | solution.py:109
  55.8 1.2 %fusion.15 = f32[16,1,64]{2,1,0:T(1,128)S(1)} fusion(bf16[16,128,1]{1,2,0:T(2,128)(2,1)S(1)} %reshape.394, bf16[64,16,128]{2,1,0:T(8,128)(2,1)} %param.14), kind=kOutput, calls=%fused_computation.153 | convolution fusion | flops 262144 | bytes 270336 | tf_op jit(solution)/shard_map/shd,chd->shc/dot_general | solution.py:131
  57.5 11.4 %all-to-all-done = bf16[128,2,1024]{2,1,0:T(2,128)(2,1)} async-done(((bf16[128,2,1024]{2,1,0:T(2,128)(2,1)}), bf16[128,2,1024]{2,1,0:T(2,128)(2,1)}, u32[]{:S(2)}, u32[]{:S(2)}) %all-to-all-start) | async-done | bytes 524320 | tf_op jit(solution)/shard_map/all_to_all | solution.py:109
  68.9 2.3 %reshape.403 = bf16[128,1,1,32,64]{4,3,2,1,0:T(8,128)(2,1)S(1)} reshape(bf16[128,2,1024]{2,1,0:T(2,128)(2,1)} %all-to-all-done) | data formatting | bytes 1048576
  71.5 0.9 fusion.1
  72.4 0.6 dynamic-slice.2
  74.9 0.9 squeeze.3
  75.8 1.1 copy.674
  76.9 15.5 %all-gather.5.cloned.1.call-done = bf16[128,4096]{1,0:T(8,128)(2,1)} async-done(((bf16[16,4096]{1,0:T(8,128)(2,1)}), bf16[128,4096]{1,0:T(8,128)(2,1)}) %all-gather.5.cloned.1.call-update) | async-done | bytes 1048592 | tf_op jit(solution)/shard_map/all_gather | solution.py:32
  92.5 1.4 %convert_reduce_fusion = f32[16,4096]{1,0:T(8,128)S(1)} fusion(bf16[8,16,4096]{2,1,0:T(8,128)(2,1)} %bitcast.844), kind=kLoop, calls=%fused_computation.8 | loop fusion | flops 983040 | bytes 1310720 | tf_op jit(solution)/shard_map/reduce_sum | solution.py:33
  94.6 1.1 %fusion.13 = f32[16,1,128]{2,1,0:T(1,128)S(1)} fusion(bf16[64,16,128]{2,1,0:T(8,128)(2,1)} %param.15, bf16[16,64,1]{1,0,2:T(8,128)(2,1)S(1)} %fusion.6), kind=kOutput, calls=%fused_computation.151 | convolution fusion | flops 262144 | bytes 272384 | tf_op jit(solution)/shard_map/shc,chv->hsv/dot_general | solution.py:150
  95.7 6.9 %all-reduce = f32[16,1,128]{2,0,1:T(8,128)S(1)} all-reduce(f32[16,1,128]{2,0,1:T(8,128)S(1)} %bitcast.850), channel_id=4, replica_groups=mesh['sp'=16,'tp_0'=4,'tp_1'=2] {'tp_0'}, use_global_device_ids=true, to_apply=%region_5.0.clone | all-reduce | flops 2048 | bytes 16384
  102.6 4.4 %all-reduce.1 = f32[4,1,128]{2,0,1:T(4,128)S(1)} all-reduce(f32[4,1,128]{2,0,1:T(4,128)S(1)} %constant_dynamic-slice_fusion), channel_id=5, replica_groups=mesh['sp'=16,'tp_0'=4,'tp_1'=2] {'tp_1'}, use_global_device_ids=true, to_apply=%region_6.0.clone | all-reduce | flops 512 | bytes 4096
  107.2 0.6 multiply_convert_fusion
  (183 shorter events, 5.6 us)
Async XLA Ops:
  7.2 30.5 %copy-start = (bf16[2048,512]{1,0:T(8,128)(2,1)S(1)}, bf16[2048,512]{1,0:T(8,128)(2,1)}, u32[]{:S(2)}) copy-start(bf16[2048,512]{1,0:T(8,128)(2,1)} %param.11) | copy-start | bytes 6291460
  7.2 2.3 %copy-start.4 = (f32[2048]{0:T(1024)S(1)}, f32[2048]{0:T(1024)}, u32[]{:S(2)}) copy-start(f32[2048]{0:T(1024)} %param.10) | copy-start | bytes 24580
  7.2 2.3 %copy-start.1 = (bf16[16,32,2048]{2,1,0:T(8,128)(2,1)S(1)}, bf16[16,32,2048]{2,1,0:T(8,128)(2,1)}, u32[]{:S(2)}) copy-start(bf16[16,32,2048]{2,1,0:T(8,128)(2,1)} %param.9) | copy-start | bytes 6291460
  9.6 1.9 %copy-start.3 = (bf16[2048,64]{0,1:T(8,128)(2,1)S(1)}, bf16[2048,64]{0,1:T(8,128)(2,1)}, u32[]{:S(2)}) copy-start(bf16[2048,64]{0,1:T(8,128)(2,1)} %param.12) | copy-start | bytes 786436
  10.1 1.4 %copy-start.2 = (bf16[16,32,2048]{2,1,0:T(8,128)(2,1)}, bf16[16,32,2048]{2,1,0:T(8,128)(2,1)S(1)}, u32[]{:S(2)}) copy-start(bf16[16,32,2048]{2,1,0:T(8,128)(2,1)S(1)} %fusion.4) | copy-start | bytes 6291460
  11.5 13.8 %copy-start.7 = (bf16[1,2,64]{2,1,0:T(2,128)(2,1)S(1)}, bf16[1,2,64]{2,1,0:T(2,128)(2,1)}, u32[]{:S(2)}) copy-start(bf16[1,2,64]{2,1,0:T(2,128)(2,1)} %param.17) | copy-start | bytes 772
  11.5 13.9 %copy-start.6 = (bf16[1,2,128]{2,1,0:T(2,128)(2,1)S(1)}, bf16[1,2,128]{2,1,0:T(2,128)(2,1)}, u32[]{:S(2)}) copy-start(bf16[1,2,128]{2,1,0:T(2,128)(2,1)} %param.16) | copy-start | bytes 1540
  13.8 32.9 %all-to-all-start.1 = ((bf16[128,2,128]{2,1,0:T(2,128)(2,1)}), bf16[128,2,128]{2,1,0:T(2,128)(2,1)S(1)}, u32[]{:S(2)}, u32[]{:S(2)}) async-start(bf16[128,2,128]{2,1,0:T(2,128)(2,1)} %reshape.404), calls=%async_computation.1 | async-start | bytes 131072 | tf_op jit(solution)/shard_map/all_to_all | solution.py:121
  37.7 2.9 %copy-start.5 = (f32[512]{0:T(512)S(1)}, f32[512]{0:T(512)}, u32[]{:S(2)}) copy-start(f32[512]{0:T(512)} %param.13) | copy-start | bytes 6148
  46.7 22.2 %all-to-all-start = ((bf16[128,2,1024]{2,1,0:T(2,128)(2,1)}), bf16[128,2,1024]{2,1,0:T(2,128)(2,1)}, u32[]{:S(2)}, u32[]{:S(2)}) async-start(bf16[128,2,1024]{2,1,0:T(2,128)(2,1)} %reshape.402), calls=%async_computation | async-start | bytes 1048576 | tf_op jit(solution)/shard_map/all_to_all | solution.py:109
  55.6 36.9 %all-gather.5.cloned.1.call-start = ((), (), s32[]{:S(2)}) async-start(), calls=%async_computation.2 | async-start | bytes 1179648 | tf_op jit(solution)/shard_map/all_gather | solution.py:32
  57.2 15.3 %copy-start.9 = (u32[128]{0:T(128)S(1)}, u32[128]{0:T(128)}, u32[]{:S(2)}) copy-start(u32[128]{0:T(128)} %constant.62) | copy-start | bytes 1540
  57.2 15.9 %copy-start.8 = (u32[128]{0:T(128)S(1)}, u32[128]{0:T(128)}, u32[]{:S(2)}) copy-start(u32[128]{0:T(128)} %constant.58) | copy-start | bytes 1540
Sparse Core Ops, SparseCore 0:
  72.5 19.8 all-gather.4
